TPU v7x, 32 devices: a whole 2x2x4 slice. The times are simulated.
32 devices in a mesh: gr: 2 (over core), sp: 8 (over z, y), tp: 2 (over x).
Axes of the slice: x: 2, y: 2, z: 4, core: 2. Of those that a mesh axis runs over, the one named last changes fastest.
Arguments:
- tokens: bfloat16 [4, 2048, 2048], P('gr', ('sp', 'tp')), parts along dimension 0, may hold values from -6 to 6
- key_weight: bfloat16 [2048, 1024], P('sp'), may hold values from -0.125 to 0.125
- value_weight: bfloat16 [2048, 1024], P('sp'), may hold values from -0.125 to 0.125
- queries: bfloat16 [4, 1024], P('gr'), parts along dimension 0, may hold values from -6 to 6
- head_offset: float32 [16], replicated, may hold values from -14 to -3.5
- key_bias: bfloat16 [4, 2048, 16], P('gr', ('sp', 'tp')), parts along dimension 0, may hold values from -0.5 to 12.9
Outputs:
- key_cache: bfloat16 [4, 2048, 1024], P('gr', 'sp', 'tp'), parts along dimension 0
- value_cache: bfloat16 [4, 2048, 1024], P('gr', 'sp', 'tp'), parts along dimension 0
- bias_cache: bfloat16 [4, 2048, 16], P('gr', 'sp', 'tp'), parts along dimension 0
- reading: float32 [4, 1024], P('gr', 'tp'), parts along dimension 0
There are 2 independent parts, one for each index of `gr`. A program takes and returns all parts, laid end to end along the dimension named above; an argument that names none is the same for every part. Nothing has to cross between parts.
All inputs are finite; a program needn't handle non-finite values.
Results may differ from a plain program's by a relative error of at most 0.0052.
Values may be sent and summed in bfloat16 or wider, within the bound.
A program may use at most 64 MiB of HBM per device.

v0:
```python
import jax
import jax.numpy as jnp
from jax import lax
from jax.sharding import PartitionSpec as P


def carried_in(x, axis, combine, identity):
    length, position = (lax.axis_size(axis), lax.axis_index(axis))
    everything = lax.all_gather(x, axis)
    start = jnp.broadcast_to(jnp.asarray(identity, x.dtype), x.shape)

    def lap(k, before):
        at = length - 1 - k
        reached = at > position
        new = combine(before, everything[at])
        return jnp.where(reached, new, before)

    return lax.fori_loop(0, length, lap, start)


def add_terms(earlier, later):
    return earlier + later


def normalize(mixture):
    return mixture * lax.rsqrt(jnp.mean(mixture * mixture, axis=-1, keepdims=True) + 1e-06)


def per_device(tokens, key_weight, value_weight, queries, head_offset, key_bias):
    seq_count, pos_dev, model_width = tokens.shape
    head_count = head_offset.shape[0]
    kv_width = key_weight.shape[1]
    head_dim = kv_width // head_count
    score_scale = head_dim ** (-0.5)
    tp_count = lax.axis_size("tp")
    col_width = kv_width // tp_count
    col_start = lax.axis_index("tp") * col_width
    own_cols = jnp.concatenate(
        [
            lax.dynamic_slice_in_dim(key_weight, col_start, col_width, 1),
            lax.dynamic_slice_in_dim(value_weight, col_start, col_width, 1),
        ],
        axis=1,
    )
    full_cols = lax.all_gather(own_cols, "sp", axis=0, tiled=True)
    projected = jnp.einsum(
        "spd,dw->spw",
        lax.all_gather(tokens, "tp", axis=1, tiled=True),
        full_cols,
        preferred_element_type=jnp.float32,
    ).astype(jnp.bfloat16)
    key_cache = projected[:, :, :col_width]
    value_cache = projected[:, :, col_width:]
    bias_cache = lax.all_to_all(key_bias, "tp", split_axis=2, concat_axis=1, tiled=True)
    span_len = key_cache.shape[1]
    local_heads = bias_cache.shape[2]
    key_blocks = key_cache.reshape(seq_count, span_len, local_heads, head_dim)
    value_blocks = value_cache.reshape(seq_count, span_len, local_heads, head_dim)
    query_cols = lax.dynamic_slice_in_dim(queries, col_start, col_width, 1)
    query_heads = query_cols.reshape(seq_count, local_heads, head_dim)
    head_start = lax.axis_index("tp") * local_heads
    local_offset = lax.dynamic_slice_in_dim(head_offset, head_start, local_heads, 0)
    logits = (
        jnp.einsum("sphc,shc->shp", key_blocks, query_heads, preferred_element_type=jnp.float32)
        * score_scale
    )
    logits = (
        logits
        + local_offset[None, :, None]
        + jnp.transpose(bias_cache.astype(jnp.float32), (0, 2, 1))
    )
    fading = jax.nn.log_sigmoid(-logits)
    within = lax.cumsum(fading, axis=2, reverse=True) - fading
    block_total = jnp.sum(fading, axis=2)
    carried = carried_in(block_total, "sp", add_terms, jnp.zeros_like(block_total))
    weights = jnp.exp(jax.nn.log_sigmoid(logits) + within + carried[:, :, None]).astype(
        jnp.bfloat16
    )
    partial_value = jnp.einsum(
        "shp,sphc->shc", weights, value_blocks, preferred_element_type=jnp.float32
    )
    mixture = lax.psum(partial_value, "sp")
    reading = normalize(mixture).reshape(seq_count, col_width)
    return (key_cache, value_cache, bias_cache, reading)


def solution(mesh):
    in_specs = (
        P("gr", ("sp", "tp"), None),
        P("sp", None),
        P("sp", None),
        P("gr", None),
        P(),
        P("gr", ("sp", "tp"), None),
    )
    out_specs = (P("gr", "sp", "tp"), P("gr", "sp", "tp"), P("gr", "sp", "tp"), P("gr", "tp"))
    return jax.shard_map(
        per_device, mesh=mesh, in_specs=in_specs, out_specs=out_specs, check_vma=False
    )
```

profile of v0, /device:TPU:0, one launch (start us, length us, event | category | flops | bytes accessed | tf_op | source)
XLA Modules:
  0.0 179.6 jit_solution(294673093222609058)
XLA Ops:
  7.2 0.0 copy-start
  7.2 0.0 all-gather.7.cloned.1.call-start
  7.2 0.7 all-gather.7.cloned.1.call-update
  7.9 0.0 copy-start.2
  7.9 0.0 copy-start.3
  7.9 0.0 all-gather.5.cloned.1.call-start
  8.0 1.1 constant_dynamic-slice_fusion.1
  9.1 0.1 copy.28
  9.2 0.1 copy.29
  9.3 0.8 pad_maximum_fusion
  10.2 0.0 all-gather.5.cloned.1.call-update
  10.2 0.0 copy-done.2
  10.2 0.6 copy.20
  10.8 4.2 %all-to-all-start = ((bf16[2,128,16]{1,0,2:T(2,128)(2,1)}), bf16[2,128,16]{1,0,2:T(2,128)(2,1)S(1)}, u32[]{:S(2)}, u32[]{:S(2)}) async-start(bf16[2,128,16]{1,0,2:T(2,128)(2,1)} %copy.20), calls=%async_computation | async-start | bytes 16384 | tf_op jit(solution)/shard_map/all_to_all | solution.py:54
  15.0 0.0 copy-done
  15.1 0.1 reshape.64
  15.1 0.0 copy-done.3
  15.1 0.1 dynamic_slice.25
  15.2 30.2 %all-gather.7.cloned.1.call-done = bf16[2,256,2048]{2,1,0:T(8,128)(2,1)} async-done(((bf16[2,128,2048]{2,1,0:T(8,128)(2,1)}), bf16[2,256,2048]{2,1,0:T(8,128)(2,1)}) %all-gather.7.cloned.1.call-update) | async-done | bytes 2097168 | tf_op jit(solution)/shard_map/all_gather | solution.py:48
  45.4 77.3 %all-gather.5.cloned.1.call-done = bf16[2048,1024]{0,1:T(8,128)(2,1)} async-done(((bf16[256,1024]{0,1:T(8,128)(2,1)}), bf16[2048,1024]{0,1:T(8,128)(2,1)}) %all-gather.5.cloned.1.call-update) | async-done | bytes 4194320 | tf_op jit(solution)/shard_map/all_gather | solution.py:45
  122.7 5.2 %fusion.5 = bf16[2,256,1024]{1,2,0:T(8,128)(2,1)S(1)} fusion(bf16[2,256,2048]{2,1,0:T(8,128)(2,1)} %all-gather.7.cloned.1.call-done, bf16[2048,1024]{0,1:T(8,128)(2,1)} %all-gather.5.cloned.1.call-done), kind=kOutput, calls=%fused_computation.4 | convolution fusion | flops 2148007936 | bytes 7340032 | tf_op jit(solution)/shard_map/spd,dw->spw/dot_general | solution.py:46
  127.9 0.1 fusion.18
  128.0 0.2 fusion.19
  128.2 1.0 copy.22
  129.2 0.0 all-to-all-done
  129.2 0.1 negate_bitcast_fusion
  129.3 0.0 copy-start.1
  129.3 0.2 fusion.16
  129.5 17.7 %all-gather.1 = f32[8,2,8]{2,1,0:T(2,128)S(1)} all-gather(f32[1,2,8]{2,1,0:T(2,128)S(1)} %negate_bitcast_fusion.1), channel_id=2, replica_groups=mesh['gr'=2,'sp'=8,'tp'=2] {'sp'}, dimensions={0}, use_global_device_ids=true | all-gather | bytes 576 | tf_op jit(solution)/shard_map/all_gather | solution.py:9
  147.2 0.3 while.16
  147.5 5.0 %reduce-window.6 = f32[2,8,2,128]{3,1,2,0:T(8,128)S(1)} reduce-window(f32[2,8,2,128]{3,1,2,0:T(8,128)S(1)} %get-tuple-element.150, f32[]{:T(128)} %constant.72.clone.1), window={size=1x1x1x128 pad=0_0x0_0x0_0x0_127}, to_apply=%region_0.1 | reduce-window | flops 520192 | bytes 32772 | tf_op jit(solution)/shard_map/reduce-window
  152.5 0.1 slice_reduce_fusion
  152.6 1.0 copy.23
  153.6 0.1 fusion.17
  153.7 0.2 fusion.14
  153.9 17.9 %psum.7 = f32[2,8,64]{2,1,0:T(8,128)S(1)} all-reduce(f32[2,8,64]{2,1,0:T(8,128)S(1)} %bitcast.62), channel_id=1, replica_groups=mesh['gr'=2,'sp'=8,'tp'=2] {'sp'}, use_global_device_ids=true, to_apply=%region_5.6 | all-reduce | flops 1024 | bytes 8192 | tf_op jit(solution)/shard_map/psum | solution.py:82
  171.9 0.1 multiply_reduce_fusion
  172.0 0.1 broadcast_multiply_fusion
  172.1 0.7 reshape.53
  172.7 0.0 copy-done.1
  (14 shorter events, 0.2 us)
Async XLA Ops:
  7.2 7.9 %copy-start = (bf16[2,1024]{1,0:T(2,128)(2,1)S(1)}, bf16[2,1024]{1,0:T(2,128)(2,1)}, u32[]{:S(2)}) copy-start(bf16[2,1024]{1,0:T(2,128)(2,1)} %param.11) | copy-start | bytes 12292
  7.2 38.2 %all-gather.7.cloned.1.call-start = ((), (), s32[]{:S(2)}) async-start(), calls=%async_computation.2 | async-start | bytes 3145728 | tf_op jit(solution)/shard_map/all_gather | solution.py:48
  7.9 2.3 %copy-start.2 = (bf16[2,128,16]{1,2,0:T(8,128)(2,1)S(1)}, bf16[2,128,16]{1,2,0:T(8,128)(2,1)}, u32[]{:S(2)}) copy-start(bf16[2,128,16]{1,2,0:T(8,128)(2,1)} %param.13) | copy-start | bytes 24580
  7.9 7.2 %copy-start.3 = (f32[16]{0:T(128)S(1)}, f32[16]{0:T(128)}, u32[]{:S(2)}) copy-start(f32[16]{0:T(128)} %param.12) | copy-start | bytes 196
  7.9 114.7 %all-gather.5.cloned.1.call-start = ((), (), s32[]{:S(2)}) async-start(), calls=%async_computation.1 | async-start | bytes 4718592 | tf_op jit(solution)/shard_map/all_gather | solution.py:45
  10.8 118.4 %all-to-all-start = ((bf16[2,128,16]{1,0,2:T(2,128)(2,1)}), bf16[2,128,16]{1,0,2:T(2,128)(2,1)S(1)}, u32[]{:S(2)}, u32[]{:S(2)}) async-start(bf16[2,128,16]{1,0,2:T(2,128)(2,1)} %copy.20), calls=%async_computation | async-start | bytes 16384 | tf_op jit(solution)/shard_map/all_to_all | solution.py:54
  129.3 43.5 %copy-start.1 = (bf16[2,256,8]{1,2,0:T(8,128)(2,1)}, bf16[2,256,8]{1,2,0:T(8,128)(2,1)S(1)}, u32[]{:S(2)}) copy-start(bf16[2,256,8]{1,2,0:T(8,128)(2,1)S(1)} %get-tuple-element.151) | copy-start | bytes 24580
Sparse Core Ops, SparseCore 0:
  9.5 35.8 all-gather.6
  48.0 74.6 all-gather.4
where the time goes:
time: 180 us
  waiting for transfers between devices  108 us (60%)
  blocking collectives  35.7 us (20%)
  between operations  14.2 us (8%)
  other arithmetic  6.49 us (4%)
  matrix products  5.64 us (3%)
  local copies, waits for them, and re-layouts  4.99 us (3%)
  starting transfers between devices  4.31 us (2%)
    all_gather x1, waiting for transfers between devices, per_device(): full_cols = lax.all_gather(own_cols, 'sp', axis=0, tiled=True)  77.3 us
    all_gather x1, waiting for transfers between devices, per_device(): lax.all_gather(tokens, 'tp', axis=1, tiled=True)  30.2 us
    psum x1, blocking collectives, per_device(): mixture = lax.psum(partial_value, 'sp')  17.9 us
    all_gather x1, blocking collectives, carried_in(): everything = lax.all_gather(x, axis)  17.7 us
    dot_general x1, matrix products, per_device(): jnp.einsum('spd,dw->spw', lax.all_gather(tokens, 'tp', axis=1, tiled=True...  5.22 us
    another operation x2, other arithmetic  5.02 us
    all_to_all x1, starting transfers between devices, per_device(): lax.all_to_all(key_bias, 'tp', split_axis=2, concat_axis=1, tiled=True)  4.23 us
  transfers between devices with their start and end apart: 3, of which 2 were waited for; matrix products, arithmetic and copies ran while one was open for 5% of the time, Pallas kernels for 0%

commit v1 on v0

--- a/solution.py
+++ b/solution.py
@@ -79,7 +79,9 @@
     partial_value = jnp.einsum(
         "shp,sphc->shc", weights, value_blocks, preferred_element_type=jnp.float32
     )
-    mixture = lax.psum(partial_value, "sp")
+    mixture = partial_value
+    for hop in (1, 2, 4):
+        mixture = mixture + lax.ppermute(mixture, "sp", [(dev, dev ^ hop) for dev in range(8)])
     reading = normalize(mixture).reshape(seq_count, col_width)
     return (key_cache, value_cache, bias_cache, reading)
 

time: 180 us -> 172 us (0.956)
  blocking collectives: 35.7 us -> 17.7 us
  waiting for transfers between devices: 108 us -> 117 us
    psum x1 -> x0, blocking collectives: 17.9 us -> none  [per_device(): mixture = lax.psum(partial_value, 'sp')]
    ppermute x0 -> x3, waiting for transfers between devices: none -> 9.26 us  [per_device(): lax.ppermute(mixture, 'sp', [(dev, dev ^ hop) for dev in range(8)])]
  transfers between devices with their start and end apart: 3 -> 6, of which waited for: 2 -> 5; matrix products, arithmetic and copies ran while one was open for 5% -> 6% of each run, Pallas kernels for 0% -> 0%
where the time goes in v1:
time: 172 us
  waiting for transfers between devices  117 us (68%)
  blocking collectives  17.7 us (10%)
  between operations  14.2 us (8%)
  other arithmetic  6.51 us (4%)
  matrix products  5.64 us (3%)
  local copies, waits for them, and re-layouts  4.98 us (3%)
  starting transfers between devices  4.9 us (3%)
    all_gather x1, waiting for transfers between devices, per_device(): full_cols = lax.all_gather(own_cols, 'sp', axis=0, tiled=True)  77.3 us
    all_gather x1, waiting for transfers between devices, per_device(): lax.all_gather(tokens, 'tp', axis=1, tiled=True)  30.2 us
    all_gather x1, blocking collectives, carried_in(): everything = lax.all_gather(x, axis)  17.7 us
    ppermute x3, waiting for transfers between devices, per_device(): lax.ppermute(mixture, 'sp', [(dev, dev ^ hop) for dev in range(8)])  9.26 us
    dot_general x1, matrix products, per_device(): jnp.einsum('spd,dw->spw', lax.all_gather(tokens, 'tp', axis=1, tiled=True...  5.23 us
    another operation x2, other arithmetic  5.02 us
    all_to_all x1, starting transfers between devices, per_device(): lax.all_to_all(key_bias, 'tp', split_axis=2, concat_axis=1, tiled=True)  4.23 us
  transfers between devices with their start and end apart: 6, of which 5 were waited for; matrix products, arithmetic and copies ran while one was open for 6% of the time, Pallas kernels for 0%

profile of v1, /device:TPU:0, one launch (start us, length us, event | category | flops | bytes accessed | tf_op | source)
XLA Modules:
  0.0 171.5 jit_solution(9571162010687550313)
XLA Ops:
  7.2 0.0 copy-start
  7.2 0.0 all-gather.7.cloned.1.call-start
  7.2 0.7 all-gather.7.cloned.1.call-update
  7.9 0.0 copy-start.2
  7.9 0.0 copy-start.3
  7.9 0.0 all-gather.5.cloned.1.call-start
  8.0 1.1 constant_dynamic-slice_fusion.1
  9.1 0.1 copy.28
  9.2 0.1 copy.29
  9.3 0.8 pad_maximum_fusion
  10.2 0.0 all-gather.5.cloned.1.call-update
  10.2 0.0 copy-done.2
  10.2 0.6 copy.20
  10.8 4.2 %all-to-all-start = ((bf16[2,128,16]{1,0,2:T(2,128)(2,1)}), bf16[2,128,16]{1,0,2:T(2,128)(2,1)S(1)}, u32[]{:S(2)}, u32[]{:S(2)}) async-start(bf16[2,128,16]{1,0,2:T(2,128)(2,1)} %copy.20), calls=%async_computation | async-start | bytes 16384 | tf_op jit(solution)/shard_map/all_to_all | solution.py:54
  15.0 0.0 copy-done
  15.1 0.1 reshape.64
  15.1 0.0 copy-done.3
  15.1 0.1 dynamic_slice.25
  15.2 30.2 %all-gather.7.cloned.1.call-done = bf16[2,256,2048]{2,1,0:T(8,128)(2,1)} async-done(((bf16[2,128,2048]{2,1,0:T(8,128)(2,1)}), bf16[2,256,2048]{2,1,0:T(8,128)(2,1)}) %all-gather.7.cloned.1.call-update) | async-done | bytes 2097168 | tf_op jit(solution)/shard_map/all_gather | solution.py:48
  45.4 77.3 %all-gather.5.cloned.1.call-done = bf16[2048,1024]{0,1:T(8,128)(2,1)} async-done(((bf16[256,1024]{0,1:T(8,128)(2,1)}), bf16[2048,1024]{0,1:T(8,128)(2,1)}) %all-gather.5.cloned.1.call-update) | async-done | bytes 4194320 | tf_op jit(solution)/shard_map/all_gather | solution.py:45
  122.7 5.2 %fusion.5 = bf16[2,256,1024]{1,2,0:T(8,128)(2,1)S(1)} fusion(bf16[2,256,2048]{2,1,0:T(8,128)(2,1)} %all-gather.7.cloned.1.call-done, bf16[2048,1024]{0,1:T(8,128)(2,1)} %all-gather.5.cloned.1.call-done), kind=kOutput, calls=%fused_computation.4 | convolution fusion | flops 2148007936 | bytes 7340032 | tf_op jit(solution)/shard_map/spd,dw->spw/dot_general | solution.py:46
  127.9 0.1 fusion.18
  128.0 0.2 fusion.19
  128.2 0.0 all-to-all-done
  128.2 0.1 negate_bitcast_fusion
  128.3 0.0 copy-start.1
  128.3 0.2 fusion.16
  128.5 17.7 %all-gather.1 = f32[8,2,8]{2,1,0:T(2,128)S(1)} all-gather(f32[1,2,8]{2,1,0:T(2,128)S(1)} %negate_bitcast_fusion.1), channel_id=2, replica_groups=mesh['gr'=2,'sp'=8,'tp'=2] {'sp'}, dimensions={0}, use_global_device_ids=true | all-gather | bytes 576 | tf_op jit(solution)/shard_map/all_gather | solution.py:9
  146.2 0.3 while.16
  146.5 5.0 %reduce-window.6 = f32[2,8,2,128]{3,1,2,0:T(8,128)S(1)} reduce-window(f32[2,8,2,128]{3,1,2,0:T(8,128)S(1)} %get-tuple-element.152, f32[]{:T(128)} %constant.72.clone.1), window={size=1x1x1x128 pad=0_0x0_0x0_0x0_127}, to_apply=%region_0.1 | reduce-window | flops 520192 | bytes 32772 | tf_op jit(solution)/shard_map/reduce-window
  151.5 0.1 slice_reduce_fusion
  151.6 0.1 fusion.17
  151.7 0.2 fusion.14
  151.9 0.6 collective-permute-start
  152.5 3.1 %collective-permute-done = f32[2,8,64]{2,1,0:T(8,128)S(1)} collective-permute-done((f32[2,8,64]{2,1,0:T(8,128)S(1)}, f32[2,8,64]{2,1,0:T(8,128)S(1)}, u32[]{:S(2)}, u32[]{:S(2)}) %collective-permute-start) | collective-permute-done | bytes 4128 | tf_op jit(solution)/shard_map/ppermute | solution.py:84
  155.6 0.0 collective-permute-start.1
  155.6 3.6 %collective-permute-done.1 = f32[2,8,64]{2,1,0:T(8,128)S(1)} collective-permute-done((f32[2,8,64]{2,1,0:T(8,128)S(1)}, f32[2,8,64]{2,1,0:T(8,128)S(1)}, u32[]{:S(2)}, u32[]{:S(2)}) %collective-permute-start.1) | collective-permute-done | bytes 4128 | tf_op jit(solution)/shard_map/ppermute | solution.py:84
  159.3 0.0 collective-permute-start.2
  159.3 1.0 copy.22
  160.3 1.0 copy.23
  161.3 2.5 %collective-permute-done.2 = f32[2,8,64]{2,1,0:T(8,128)S(1)} collective-permute-done((f32[2,8,64]{2,1,0:T(8,128)S(1)}, f32[2,8,64]{2,1,0:T(8,128)S(1)}, u32[]{:S(2)}, u32[]{:S(2)}) %collective-permute-start.2) | collective-permute-done | bytes 4128 | tf_op jit(solution)/shard_map/ppermute | solution.py:84
  163.8 0.1 multiply_reduce_fusion
  163.9 0.1 broadcast_multiply_fusion
  164.0 0.7 reshape.53
  164.7 0.0 copy-done.1
  (16 shorter events, 0.2 us)
Async XLA Ops:
  7.2 7.9 %copy-start = (bf16[2,1024]{1,0:T(2,128)(2,1)S(1)}, bf16[2,1024]{1,0:T(2,128)(2,1)}, u32[]{:S(2)}) copy-start(bf16[2,1024]{1,0:T(2,128)(2,1)} %param.11) | copy-start | bytes 12292
  7.2 38.2 %all-gather.7.cloned.1.call-start = ((), (), s32[]{:S(2)}) async-start(), calls=%async_computation.2 | async-start | bytes 3145728 | tf_op jit(solution)/shard_map/all_gather | solution.py:48
  7.9 2.3 %copy-start.2 = (bf16[2,128,16]{1,2,0:T(8,128)(2,1)S(1)}, bf16[2,128,16]{1,2,0:T(8,128)(2,1)}, u32[]{:S(2)}) copy-start(bf16[2,128,16]{1,2,0:T(8,128)(2,1)} %param.13) | copy-start | bytes 24580
  7.9 7.2 %copy-start.3 = (f32[16]{0:T(128)S(1)}, f32[16]{0:T(128)}, u32[]{:S(2)}) copy-start(f32[16]{0:T(128)} %param.12) | copy-start | bytes 196
  7.9 114.7 %all-gather.5.cloned.1.call-start = ((), (), s32[]{:S(2)}) async-start(), calls=%async_computation.1 | async-start | bytes 4718592 | tf_op jit(solution)/shard_map/all_gather | solution.py:45
  10.8 117.4 %all-to-all-start = ((bf16[2,128,16]{1,0,2:T(2,128)(2,1)}), bf16[2,128,16]{1,0,2:T(2,128)(2,1)S(1)}, u32[]{:S(2)}, u32[]{:S(2)}) async-start(bf16[2,128,16]{1,0,2:T(2,128)(2,1)} %copy.20), calls=%async_computation | async-start | bytes 16384 | tf_op jit(solution)/shard_map/all_to_all | solution.py:54
  128.3 36.4 %copy-start.1 = (bf16[2,256,8]{1,2,0:T(8,128)(2,1)}, bf16[2,256,8]{1,2,0:T(8,128)(2,1)S(1)}, u32[]{:S(2)}) copy-start(bf16[2,256,8]{1,2,0:T(8,128)(2,1)S(1)} %get-tuple-element.153) | copy-start | bytes 24580
  151.9 3.7 %collective-permute-start = (f32[2,8,64]{2,1,0:T(8,128)S(1)}, f32[2,8,64]{2,1,0:T(8,128)S(1)}, u32[]{:S(2)}, u32[]{:S(2)}) collective-permute-start(f32[2,8,64]{2,1,0:T(8,128)S(1)} %bitcast.62), channel_id=1, source_target_pairs={{0,2},{2,0},{4,6},{6,4},{8,10},{10,8},{12,14},{14,12},{1,3},{3,1},... | collective-permute-start | bytes 12296 | tf_op jit(solution)/shard_map/ppermute | solution.py:84
  155.6 3.7 %collective-permute-start.1 = (f32[2,8,64]{2,1,0:T(8,128)S(1)}, f32[2,8,64]{2,1,0:T(8,128)S(1)}, u32[]{:S(2)}, u32[]{:S(2)}) collective-permute-start(f32[2,8,64]{2,1,0:T(8,128)S(1)} %add.105), channel_id=1, source_target_pairs={{0,4},{2,6},{4,0},{6,2},{8,12},{10,14},{12,8},{14,10},{1,5},{3,7},... | collective-permute-start | bytes 12296 | tf_op jit(solution)/shard_map/ppermute | solution.py:84
  159.3 4.5 %collective-permute-start.2 = (f32[2,8,64]{2,1,0:T(8,128)S(1)}, f32[2,8,64]{2,1,0:T(8,128)S(1)}, u32[]{:S(2)}, u32[]{:S(2)}) collective-permute-start(f32[2,8,64]{2,1,0:T(8,128)S(1)} %add.106), channel_id=1, source_target_pairs={{0,8},{2,10},{4,12},{6,14},{8,0},{10,2},{12,4},{14,6},{1,9},{3,11}... | collective-permute-start | bytes 12296 | tf_op jit(solution)/shard_map/ppermute | solution.py:84
Sparse Core Ops, SparseCore 0:
  9.5 35.8 all-gather.6
  48.0 74.6 all-gather.4
